TPU v7x, 128 devices: a whole 4x4x4 slice. The times are simulated.
128 devices in a mesh: sp: 64 (over z, y, x), tp: 2 (over core).
Axes of the slice: x: 4, y: 4, z: 4, core: 2. Of those that a mesh axis runs over, the one named last changes fastest.
Arguments:
- residual: bfloat16 [16384, 2048], P(('sp', 'tp')), may hold values from -6 to 6
- queries: bfloat16 [16384, 1152], P('sp', 'tp'), may hold values from -800 to 800
- latent: bfloat16 [16384, 256], P('sp'), may hold values from -6 to 6
- rope_key: bfloat16 [16384, 32], P('sp'), may hold values from -6 to 6
- doc_ids: int32 [16384], P('sp'), may hold values from 0 to 5, never falling along the last dimension, each value on 1 to 8192 neighbouring positions
- latent_to_key: bfloat16 [256, 768], P(None, 'tp'), may hold values from -0.375 to 0.375
- latent_to_value: bfloat16 [256, 768], P(None, 'tp'), may hold values from -0.375 to 0.375
- out_proj: bfloat16 [768, 2048], replicated, may hold values from -0.21875 to 0.21875
- mix_gain: float32 [2048], replicated, may hold values from 0.1 to 1.9
- moe_gain: float32 [2048], replicated, may hold values from 0.1 to 1.9
- expert_ids: int32 [16384, 2], P(('sp', 'tp')), may hold values from 0 to 63, as said below
- route_weight: float32 [16384, 2], P(('sp', 'tp')), may hold values from 0.1 to 1
- gate_weight: bfloat16 [64, 2048, 1024], P('sp', None, 'tp'), may hold values from -0.125 to 0.125
- up_weight: bfloat16 [64, 2048, 1024], P('sp', None, 'tp'), may hold values from -0.125 to 0.125
- down_weight: bfloat16 [64, 1024, 2048], P('sp', 'tp'), may hold values from -0.1875 to 0.1875
Outputs:
- output: bfloat16 [16384, 2048], P(('sp', 'tp'))
Inputs may be any that keep to these rules, and one draw needn't show every extreme that they name: `expert_ids`: each row names 2 different experts of one group of 16 consecutive numbers; in each aligned block of 128 rows (the rows of one device) no expert is named more than 8 times, and some expert exactly 8 times.
All inputs are finite; a program needn't handle non-finite values.
Results may differ from a plain program's by a relative error of at most 0.013.
Values may be sent and summed in bfloat16 or wider, within the bound.
A program may use at most 64 MiB of HBM per device.

v0:
```python
import math
import jax
import jax.numpy as jnp
from jax import lax
from jax.sharding import PartitionSpec as P

D = 2048
UNROTATED_DIM = 64
ROPE = 32
VALUE_ENTRIES = 64
GROUPS = 4
rope_base = 10000.0
epsilon = 1e-06


def in_order(pieces, dim):
    pieces = jnp.moveaxis(pieces, 0, dim)
    lengths = pieces.shape
    return pieces.reshape(*lengths[:dim], lengths[dim] * lengths[dim + 1], *lengths[dim + 2 :])


def sent_to_all(x, axis):
    size = lax.axis_size(axis)
    return lax.all_to_all(jnp.broadcast_to(x[None], (size, *x.shape)), axis, 0, 0, tiled=True)


def collect(x, axis, dim):
    return in_order(sent_to_all(x, axis), dim)


def cut_along(x, dim, size):
    before, after = (x.shape[:dim], x.shape[dim + 1 :])
    return jnp.moveaxis(x.reshape(*before, size, -1, *after), dim, 0)


def sum_at_owner(x, axis, dim):
    pieces = cut_along(x, dim, lax.axis_size(axis))
    arrived = lax.all_to_all(pieces, axis, split_axis=0, concat_axis=0, tiled=True)
    return arrived.astype(jnp.float32).sum(axis=0)


def rotate(source, positions):
    half_width = source.shape[-1] // 2
    frequency = rope_base ** (-jnp.arange(half_width, dtype=jnp.float32) / half_width)
    angles = positions.astype(jnp.float32)[:, None] * frequency[None, :]
    if source.ndim == 3:
        angles = angles[:, None, :]
    cosine = jnp.cos(angles)
    sine_part = jnp.sin(angles)
    upper_half = source[..., :half_width].astype(jnp.float32)
    lower_half = source[..., half_width:].astype(jnp.float32)
    turned = jnp.concatenate(
        [
            upper_half * cosine - lower_half * sine_part,
            lower_half * cosine + upper_half * sine_part,
        ],
        axis=-1,
    )
    return turned.astype(jnp.bfloat16)


def rms_scale(source, gain):
    return source * lax.rsqrt(jnp.mean(source * source, axis=-1, keepdims=True) + epsilon) * gain


def attend_keys(
    running,
    query_nope,
    query_rot,
    query_pos,
    query_docs,
    key_nope,
    key_rot,
    value_rows,
    key_pos,
    key_docs,
):
    row_max, row_total, weighted = running
    score_scale = (UNROTATED_DIM + ROPE) ** (-0.5)
    scores = (
        jnp.einsum("qhd,khd->qhk", query_nope, key_nope, preferred_element_type=jnp.float32)
        + jnp.einsum("qhr,kr->qhk", query_rot, key_rot, preferred_element_type=jnp.float32)
    ) * score_scale
    allowed = (
        (key_pos[None, :] <= query_pos[:, None]) & (key_docs[None, :] == query_docs[:, None])
    )[:, None, :]
    new_max = jnp.maximum(row_max, jnp.max(jnp.where(allowed, scores, -1e30), axis=-1))
    weights = jnp.where(allowed, jnp.exp(scores - new_max[..., None]), 0.0)
    factor = jnp.exp(row_max - new_max)
    row_total = row_total * factor + jnp.sum(weights, axis=-1)
    weighted = weighted * factor[..., None] + jnp.einsum(
        "qhk,khd->qhd", weights.astype(jnp.bfloat16), value_rows, preferred_element_type=jnp.float32
    )
    return (new_max, row_total, weighted)


def local(
    residual,
    queries,
    latent,
    rope_key,
    doc_ids,
    latent_to_key,
    latent_to_value,
    out_proj,
    mix_gain,
    moe_gain,
    expert_ids,
    route_weight,
    gate_weight,
    up_weight,
    down_weight,
):
    local_rows = queries.shape[0]
    local_heads = queries.shape[1] // (UNROTATED_DIM + ROPE)
    query_pos = lax.axis_index("sp") * local_rows + jnp.arange(local_rows, dtype=jnp.int32)
    shaped = queries.reshape(local_rows, local_heads, UNROTATED_DIM + ROPE)
    query_nope = shaped[..., :UNROTATED_DIM]
    query_rot = rotate(shaped[..., UNROTATED_DIM:], query_pos)
    key_rot = rotate(rope_key, query_pos)
    initial = (
        jnp.full((local_rows, local_heads), -1e30, jnp.float32),
        jnp.zeros((local_rows, local_heads), jnp.float32),
        jnp.zeros((local_rows, local_heads, VALUE_ENTRIES), jnp.float32),
    )
    pieces = (
        lax.all_gather(latent, "sp", axis=0, tiled=True),
        lax.all_gather(key_rot, "sp", axis=0, tiled=True),
        lax.all_gather(doc_ids, "sp", axis=0, tiled=True),
    )
    row_count = pieces[0].shape[0]
    block_rows = math.gcd(row_count, 512)

    def one_block(number, current):
        first_row = number * block_rows
        sliced = [lax.dynamic_slice_in_dim(member, first_row, block_rows, 0) for member in pieces]
        key_pos = first_row + jnp.arange(block_rows, dtype=jnp.int32)
        active = (first_row <= query_pos[-1]) & (sliced[-1][-1] >= doc_ids[0])

        def compute(carried):
            key_nope = jnp.dot(sliced[0], latent_to_key, preferred_element_type=jnp.float32).astype(
                jnp.bfloat16
            )
            value_rows = jnp.dot(
                sliced[0], latent_to_value, preferred_element_type=jnp.float32
            ).astype(jnp.bfloat16)
            key_part = sliced[1]
            return attend_keys(
                carried,
                query_nope,
                query_rot,
                query_pos,
                doc_ids,
                key_nope.reshape(block_rows, local_heads, UNROTATED_DIM),
                key_part,
                value_rows.reshape(block_rows, local_heads, VALUE_ENTRIES),
                key_pos,
                sliced[-1],
            )

        return lax.cond(active, compute, lambda carried: carried, current)

    running = lax.fori_loop(0, row_count // block_rows, one_block, initial)
    attended = (running[2] / running[1][..., None]).astype(jnp.bfloat16)
    attended = attended.reshape(local_rows, local_heads * VALUE_ENTRIES)
    gathered = lax.all_to_all(attended, "tp", split_axis=0, concat_axis=1, tiled=True)
    mix = jnp.dot(gathered, out_proj, preferred_element_type=jnp.float32)
    branch = rms_scale(mix, mix_gain)
    middle = lax.optimization_barrier((residual.astype(jnp.float32) + branch).astype(jnp.bfloat16))
    normed = rms_scale(middle.astype(jnp.float32), moe_gain).astype(jnp.bfloat16)
    row_count = normed.shape[0]
    top_count = expert_ids.shape[1]
    expert_count = lax.axis_size("sp")
    capacity = row_count // (expert_count // GROUPS)
    flat_ids = expert_ids.reshape(-1)
    onehot = (flat_ids[:, None] == jnp.arange(expert_count, dtype=jnp.int32)[None, :]).astype(
        jnp.int32
    )
    earlier = jnp.cumsum(onehot, axis=0) - onehot
    slot_rank = jnp.sum(earlier * onehot, axis=1)
    slot_ids = (flat_ids * capacity + slot_rank).reshape(row_count, top_count)
    chooser = jnp.any(
        jnp.arange(expert_count * capacity, dtype=jnp.int32)[:, None, None] == slot_ids[None],
        axis=2,
    ).astype(jnp.bfloat16)
    buffer = jnp.dot(chooser, normed, preferred_element_type=jnp.float32).astype(jnp.bfloat16)
    buffer = buffer.reshape(expert_count, capacity, D)
    arrived = lax.all_to_all(buffer, "sp", split_axis=0, concat_axis=0, tiled=True)
    model_width = arrived.shape[2]
    both_halves = collect(arrived, "tp", 0)
    flat_rows = both_halves.reshape(-1, model_width)
    gate_out = jnp.dot(flat_rows, gate_weight[0], preferred_element_type=jnp.float32)
    upward = jnp.dot(flat_rows, up_weight[0], preferred_element_type=jnp.float32)
    hidden = (jax.nn.silu(gate_out) * upward).astype(jnp.bfloat16)
    partial_value = jnp.dot(hidden, down_weight[0], preferred_element_type=jnp.float32).reshape(
        both_halves.shape
    )
    summed = sum_at_owner(partial_value.astype(jnp.bfloat16), "tp", 0).astype(jnp.bfloat16)
    returned = lax.all_to_all(summed, "sp", split_axis=0, concat_axis=0, tiled=True)
    picked = returned.reshape(-1, D)[slot_ids.reshape(-1)].astype(jnp.float32)
    expert_mix = jnp.sum(
        (picked * route_weight.reshape(-1)[:, None]).reshape(row_count, top_count, D), axis=1
    )
    return (middle.astype(jnp.float32) + expert_mix).astype(jnp.bfloat16)


def solution(mesh):
    in_specs = (
        P(("sp", "tp"), None),
        P("sp", "tp"),
        P("sp", None),
        P("sp", None),
        P("sp"),
        P(None, "tp"),
        P(None, "tp"),
        P(),
        P(),
        P(),
        P(("sp", "tp"), None),
        P(("sp", "tp"), None),
        P("sp", None, "tp"),
        P("sp", None, "tp"),
        P("sp", "tp", None),
    )
    out_specs = P(("sp", "tp"), None)
    return jax.shard_map(local, mesh=mesh, in_specs=in_specs, out_specs=out_specs, check_vma=False)
```

profile of v0, /device:TPU:0, one launch (start us, length us, event | category | flops | bytes accessed | tf_op | source)
XLA Modules:
  0.0 649.7 jit_solution(9027320513454528965)
XLA Ops:
  10.0 1.6 slice.54
  13.5 186.6 %all-gather = s32[64,1,256]{2,1,0:T(1,128)} all-gather(s32[1,1,256]{2,1,0:T(1,128)} %bitcast.92), channel_id=1, replica_groups=mesh['sp'=64,'tp'=2] {'sp'}, dimensions={0}, use_global_device_ids=true | all-gather | bytes 66560 | tf_op jit(solution)/shard_map/all_gather | solution.py:129
  202.9 216.7 %while.17 = (s32[]{:T(128)}, f32[256,6]{0,1:T(8,128)S(1)}, f32[256,6]{0,1:T(8,128)S(1)}, f32[256,6,64]{0,2,1:T(8,128)S(1)}, s32[256]{0:T(256)}, /*index=5*/s32[1...) while((s32[]{:T(128)}, f32[256,6]{0,1:T(8,128)S(1)}, ...), condition=%wide.region_5.6_spmd, body=%wide.region_0.5_spmd.sunk | while | flops 461835776 | bytes 21579896 | solution.py:163
  207.4 1.3 slice.70
  209.5 7.0 %conditional.2 = ((f32[256,6]{0,1:T(8,128)S(1)}, f32[256,6]{0,1:T(8,128)S(1)}, f32[256,6,64]{0,2,1:T(8,128)S(1)})) conditional(s32[]{:T(128)} %convert_element_type.177, (f32[256,6]{0,1:T(8,128)S(1)}, f32[256,6]{0,1:T(8,128)S(1)}, f32[256,6,64]{0,2,1:T(8,128)S(1)}) %tuple.50, (s32[]{:T(128)}, s32[512]{0:T(512)}, s32[256]{0:T(256)}, s32[512]{0:T(512)}, ...), branch_computations={%region_1.0_spmd, %region_2.4_spmd} | conditional | flops 461835776 | bytes 21565132 | solution.py:161
  209.5 1.3 convolution_convert_fusion.1
  210.9 1.5 fusion.16
  221.0 1.3 slice.70
  227.5 1.3 slice.70
  234.1 1.3 slice.70
  421.4 4.0 all_to_all.39
  428.0 137.1 %all_to_all.40 = bf16[64,8,2048]{2,1,0:T(8,128)(2,1)S(1)} all-to-all(bf16[64,8,2048]{2,1,0:T(8,128)(2,1)S(1)} %fusion.23), channel_id=1, replica_groups=mesh['sp'=64,'tp'=2] {'sp'}, dimensions={0} | all-to-all | bytes 4194304 | tf_op jit(solution)/shard_map/all_to_all | solution.py:188
  565.6 7.2 %all_to_all.41 = bf16[2,64,8,2048]{3,2,1,0:T(8,128)(2,1)S(1)} all-to-all(bf16[2,64,8,2048]{3,2,1,0:T(8,128)(2,1)S(1)} %broadcast_in_dim.63), channel_id=1, replica_groups=mesh['sp'=64,'tp'=2] {'tp'}, dimensions={0} | all-to-all | bytes 8388608 | tf_op jit(solution)/shard_map/all_to_all | solution.py:24
  572.8 2.3 fusion.25
  575.2 2.6 fusion.31
  577.8 2.4 convolution_convert_fusion.2
  580.8 8.2 %all_to_all.42 = bf16[2,64,8,2048]{3,1,2,0:T(8,128)(2,1)} all-to-all(bf16[2,64,8,2048]{3,1,2,0:T(8,128)(2,1)S(1)} %copy.65), channel_id=1, replica_groups=mesh['sp'=64,'tp'=2] {'tp'}, dimensions={0} | all-to-all | bytes 8388608 | tf_op jit(solution)/shard_map/all_to_all | solution.py:38
  589.0 3.5 reduce_sum.67
  592.5 2.5 copy.67
  595.0 6.1 all-to-all-start.4
  601.3 29.9 %all-to-all-done.4 = bf16[64,8,2048]{2,1,0:T(8,128)(2,1)S(1)} async-done(((bf16[64,8,2048]{2,1,0:T(8,128)(2,1)}), bf16[64,8,2048]{2,1,0:T(8,128)(2,1)S(1)}, u32[]{:S(2)}, u32[]{:S(2)}) %all-to-all-start.4) | async-done | bytes 2097184 | tf_op jit(solution)/shard_map/all_to_all | solution.py:199
  631.2 2.3 gather_fusion
  633.5 3.5 reshape.226
  637.1 4.9 multiply_reduce_fusion
  (347 shorter events, 159.0 us)
Async XLA Ops:
  6.5 418.9 %copy-start = (bf16[768,2048]{1,0:T(8,128)(2,1)S(1)}, bf16[768,2048]{1,0:T(8,128)(2,1)}, u32[]{:S(2)}) copy-start(bf16[768,2048]{1,0:T(8,128)(2,1)} %param.26) | copy-start | bytes 9437188
  6.5 196.3 %all-gather.6.cloned.1.call-start = ((), (), s32[]{:S(2)}) async-start(), calls=%async_computation.6 | async-start | bytes 1064960 | tf_op jit(solution)/shard_map/all_gather | solution.py:128
  8.2 194.6 %all-gather.4.cloned.1.call-start = ((), (), s32[]{:S(2)}) async-start(), calls=%async_computation.5 | async-start | bytes 8519680 | tf_op jit(solution)/shard_map/all_gather | solution.py:127
  12.6 190.2 %copy-start.14 = (s32[256]{0:T(256)}, s32[256]{0:T(256)S(1)}, u32[]{:S(2)}) copy-start(s32[256]{0:T(256)S(1)} %fusion.49) | copy-start | bytes 3076
  209.5 2.9 copy-start.11
  209.5 2.9 copy-start.10
  209.5 2.9 copy-start.12
  209.5 2.9 copy-start.13
  209.5 3.1 copy-start.4
  213.5 0.9 copy-start.5
  419.7 6.5 copy-start.16
  421.4 4.8 copy-start.6
  425.5 1.7 copy-start.7
  425.5 1.7 copy-start.17
  426.4 0.8 copy-start.2
  565.6 7.2 %copy-start.19 = (bf16[1,2048,512]{2,1,0:T(8,128)(2,1)S(1)}, bf16[1,2048,512]{2,1,0:T(8,128)(2,1)}, u32[]{:S(2)}) copy-start(bf16[1,2048,512]{2,1,0:T(8,128)(2,1)} %param.32) | copy-start | bytes 6291460
  572.8 2.3 copy-start.20
  575.2 2.7 copy-start.21
  595.0 6.1 copy-start.8
  595.0 6.2 copy-start.18
  595.0 6.4 copy-start.15
  595.0 36.2 %all-to-all-start.4 = ((bf16[64,8,2048]{2,1,0:T(8,128)(2,1)}), bf16[64,8,2048]{2,1,0:T(8,128)(2,1)S(1)}, u32[]{:S(2)}, u32[]{:S(2)}) async-start(bf16[64,8,2048]{2,1,0:T(8,128)(2,1)} %copy.67), calls=%async_computation.4 | async-start | bytes 4194304 | tf_op jit(solution)/shard_map/all_to_all | solution.py:199
  633.5 9.3 %copy-start.1 = (bf16[768,2048]{1,0:T(8,128)(2,1)S(1)}, bf16[768,2048]{1,0:T(8,128)(2,1)}, u32[]{:S(2)}) copy-start(bf16[768,2048]{1,0:T(8,128)(2,1)} %param.26) | copy-start | bytes 9437188
  637.1 4.9 copy-start.3
  (32 other events, 19.2 us)
Sparse Core Ops, SparseCore 0:
  10.0 66.1 all-gather.5
  79.0 76.5 all-gather.3
where the time goes:
time: 655 us; the launch traced here: 650 us
  blocking collectives  343 us (52%)
  local copies, waits for them, and re-layouts  160 us (24%)
  loops' own time  64.4 us (10%)
  waiting for transfers between devices  30.6 us (5%)
  other arithmetic  17 us (3%)
  matrix products  14.5 us (2%)
  between operations  13.7 us (2%)
    all_gather x1, blocking collectives, local(): lax.all_gather(doc_ids, 'sp', axis=0, tiled=True)  187 us
    all_to_all x1, blocking collectives, local(): lax.all_to_all(buffer, 'sp', split_axis=0, concat_axis=0, tiled=True)  137 us
    slice x96, local copies, waits for them, and re-layouts, one_block(): active = (first_row <= query_pos[-1]) & (sliced[-1][-1] >= doc_ids[0])  102 us
    another operation x1, loops' own time, local(): running = lax.fori_loop(0, row_count // block_rows, one_block, initial)  63.9 us
    all_to_all x1, waiting for transfers between devices, local(): lax.all_to_all(summed, 'sp', split_axis=0, concat_axis=0, tiled=True)  29.9 us
    dynamic_slice x32, local copies, waits for them, and re-layouts, one_block(): lax.dynamic_slice_in_dim(member, first_row, block_rows, 0)  24.2 us
    iota x32, local copies, waits for them, and re-layouts, one_block(): key_pos = first_row + jnp.arange(block_rows, dtype=jnp.int32)  19.1 us
  transfers between devices with their start and end apart: 3, of which 1 were waited for; matrix products, arithmetic and copies ran while one was open for 1% of the time, Pallas kernels for 0%

commit v1 on v0

--- a/solution.py
+++ b/solution.py
@@ -11,6 +11,11 @@
 GROUPS = 4
 rope_base = 10000.0
 epsilon = 1e-06
+
+
+def tiled_gather(x, axis, dim):
+    copies = jnp.concatenate([x] * lax.axis_size(axis), axis=dim)
+    return lax.all_to_all(copies, axis, dim, dim, tiled=True)
 
 
 def in_order(pieces, dim):
@@ -126,7 +131,7 @@
     pieces = (
         lax.all_gather(latent, "sp", axis=0, tiled=True),
         lax.all_gather(key_rot, "sp", axis=0, tiled=True),
-        lax.all_gather(doc_ids, "sp", axis=0, tiled=True),
+        tiled_gather(doc_ids, "sp", 0),
     )
     row_count = pieces[0].shape[0]
     block_rows = math.gcd(row_count, 512)

time: 655 us -> 607 us (0.927)
  blocking collectives: 343 us -> 163 us
  waiting for transfers between devices: 30.6 us -> 157 us
  starting transfers between devices: 6.11 us -> 17.6 us
    all_gather x1 -> x0, blocking collectives: 187 us -> none  [local(): lax.all_gather(doc_ids, 'sp', axis=0, tiled=True)]
    all_gather x1, waiting for transfers between devices: 0.01 us -> 79.3 us  [local(): lax.all_gather(latent, 'sp', axis=0, tiled=True)]
    all_gather x1, waiting for transfers between devices: 0.01 us -> 44.8 us  [local(): lax.all_gather(key_rot, 'sp', axis=0, tiled=True)]
    all_to_all x0 -> x1, starting transfers between devices: none -> 11.5 us  [tiled_gather(): return lax.all_to_all(copies, axis, dim, dim, tiled=True)]
  transfers between devices with their start and end apart: 3 -> 4, of which waited for: 1 -> 4; matrix products, arithmetic and copies ran while one was open for 1% -> 1% of each run, Pallas kernels for 0% -> 0%
where the time goes in v1:
time: 607 us; the launch traced here: 601 us
  blocking collectives  163 us (27%)
  local copies, waits for them, and re-layouts  158 us (26%)
  waiting for transfers between devices  157 us (26%)
  loops' own time  60.8 us (10%)
  starting transfers between devices  17.6 us (3%)
  other arithmetic  16.9 us (3%)
  matrix products  14.5 us (2%)
  between operations  13.7 us (2%)
    all_to_all x1, blocking collectives, local(): lax.all_to_all(buffer, 'sp', split_axis=0, concat_axis=0, tiled=True)  143 us
    slice x96, local copies, waits for them, and re-layouts, one_block(): active = (first_row <= query_pos[-1]) & (sliced[-1][-1] >= doc_ids[0])  99 us
    all_gather x1, waiting for transfers between devices, local(): lax.all_gather(latent, 'sp', axis=0, tiled=True)  79.3 us
    another operation x1, loops' own time, local(): running = lax.fori_loop(0, row_count // block_rows, one_block, initial)  60.3 us
    all_gather x1, waiting for transfers between devices, local(): lax.all_gather(key_rot, 'sp', axis=0, tiled=True)  44.8 us
    all_to_all x1, waiting for transfers between devices, local(): lax.all_to_all(summed, 'sp', split_axis=0, concat_axis=0, tiled=True)  29.9 us
    dynamic_slice x32, local copies, waits for them, and re-layouts, one_block(): lax.dynamic_slice_in_dim(member, first_row, block_rows, 0)  24.2 us
    iota x32, local copies, waits for them, and re-layouts, one_block(): key_pos = first_row + jnp.arange(block_rows, dtype=jnp.int32)  18.9 us
  transfers between devices with their start and end apart: 4, of which 4 were waited for; matrix products, arithmetic and copies ran while one was open for 1% of the time, Pallas kernels for 0%

profile of v1, /device:TPU:0, one launch (start us, length us, event | category | flops | bytes accessed | tf_op | source)
XLA Modules:
  0.0 601.5 jit_solution(3958371682289738184)
XLA Ops:
  9.0 1.3 concatenate.12
  10.3 11.5 %all-to-all-start = ((s32[64,256,1]{1,2,0:T(1,128)}), s32[64,256,1]{1,2,0:T(1,128)S(1)}, u32[]{:S(2)}, u32[]{:S(2)}) async-start(s32[64,256,1]{1,2,0:T(1,128)} %concatenate.12), calls=%async_computation | async-start | bytes 131072 | tf_op jit(solution)/shard_map/all_to_all | solution.py:18
  22.9 1.6 slice.54
  29.1 2.3 all-to-all-done
  31.4 44.8 %all-gather.5.cloned.1.call-done = bf16[16384,32]{0,1:T(8,128)(2,1)} async-done(((bf16[256,32]{0,1:T(8,128)(2,1)}), bf16[16384,32]{0,1:T(8,128)(2,1)}) %all-gather.5.cloned.1.call-update) | async-done | bytes 1048592 | tf_op jit(solution)/shard_map/all_gather | solution.py:133
  76.2 79.3 %all-gather.3.cloned.1.call-done = bf16[16384,256]{1,0:T(8,128)(2,1)} async-done(((bf16[256,256]{1,0:T(8,128)(2,1)}), bf16[16384,256]{1,0:T(8,128)(2,1)}) %all-gather.3.cloned.1.call-update) | async-done | bytes 8388624 | tf_op jit(solution)/shard_map/all_gather | solution.py:132
  155.6 209.8 %while.17 = (s32[]{:T(128)}, f32[256,6]{0,1:T(8,128)S(1)}, f32[256,6]{0,1:T(8,128)S(1)}, f32[256,6,64]{0,2,1:T(8,128)S(1)}, s32[256]{0:T(256)}, /*index=5*/s32[1...) while((s32[]{:T(128)}, f32[256,6]{0,1:T(8,128)S(1)}, ...), condition=%wide.region_5.6_spmd, body=%wide.region_0.5_spmd.sunk | while | flops 461835776 | bytes 21579896 | solution.py:168
  161.9 7.0 %conditional.2 = ((f32[256,6]{0,1:T(8,128)S(1)}, f32[256,6]{0,1:T(8,128)S(1)}, f32[256,6,64]{0,2,1:T(8,128)S(1)})) conditional(s32[]{:T(128)} %convert_element_type.177, (f32[256,6]{0,1:T(8,128)S(1)}, f32[256,6]{0,1:T(8,128)S(1)}, f32[256,6,64]{0,2,1:T(8,128)S(1)}) %tuple.50, (s32[]{:T(128)}, s32[512]{0:T(512)}, s32[256]{0:T(256)}, s32[512]{0:T(512)}, ...), branch_computations={%region_1.0_spmd, %region_2.4_spmd} | conditional | flops 461835776 | bytes 21565132 | solution.py:166
  162.0 1.3 convolution_convert_fusion.1
  163.3 1.5 fusion.16
  367.1 4.0 all_to_all.48
  373.7 143.2 %all_to_all.49 = bf16[64,8,2048]{2,1,0:T(8,128)(2,1)S(1)} all-to-all(bf16[64,8,2048]{2,1,0:T(8,128)(2,1)S(1)} %fusion.23), channel_id=1, replica_groups=mesh['sp'=64,'tp'=2] {'sp'}, dimensions={0} | all-to-all | bytes 4194304 | tf_op jit(solution)/shard_map/all_to_all | solution.py:193
  517.4 7.2 %all_to_all.50 = bf16[2,64,8,2048]{3,2,1,0:T(8,128)(2,1)S(1)} all-to-all(bf16[2,64,8,2048]{3,2,1,0:T(8,128)(2,1)S(1)} %broadcast_in_dim.63), channel_id=1, replica_groups=mesh['sp'=64,'tp'=2] {'tp'}, dimensions={0} | all-to-all | bytes 8388608 | tf_op jit(solution)/shard_map/all_to_all | solution.py:29
  524.7 2.3 fusion.25
  527.0 2.6 fusion.31
  529.7 2.4 convolution_convert_fusion.2
  532.6 8.2 %all_to_all.51 = bf16[2,64,8,2048]{3,1,2,0:T(8,128)(2,1)} all-to-all(bf16[2,64,8,2048]{3,1,2,0:T(8,128)(2,1)S(1)} %copy.65), channel_id=1, replica_groups=mesh['sp'=64,'tp'=2] {'tp'}, dimensions={0} | all-to-all | bytes 8388608 | tf_op jit(solution)/shard_map/all_to_all | solution.py:43
  540.8 3.5 reduce_sum.67
  544.3 2.5 copy.67
  546.8 6.1 %all-to-all-start.5 = ((bf16[64,8,2048]{2,1,0:T(8,128)(2,1)}), bf16[64,8,2048]{2,1,0:T(8,128)(2,1)S(1)}, u32[]{:S(2)}, u32[]{:S(2)}) async-start(bf16[64,8,2048]{2,1,0:T(8,128)(2,1)} %copy.67), calls=%async_computation.5 | async-start | bytes 4194304 | tf_op jit(solution)/shard_map/all_to_all | solution.py:204
  553.1 29.9 %all-to-all-done.5 = bf16[64,8,2048]{2,1,0:T(8,128)(2,1)S(1)} async-done(((bf16[64,8,2048]{2,1,0:T(8,128)(2,1)}), bf16[64,8,2048]{2,1,0:T(8,128)(2,1)S(1)}, u32[]{:S(2)}, u32[]{:S(2)}) %all-to-all-start.5) | async-done | bytes 2097184 | tf_op jit(solution)/shard_map/all_to_all | solution.py:204
  583.0 2.3 gather_fusion
  585.3 3.5 reshape.294
  588.9 4.9 multiply_reduce_fusion
  (351 shorter events, 161.0 us)
Async XLA Ops:
  6.5 364.6 %copy-start = (bf16[768,2048]{1,0:T(8,128)(2,1)S(1)}, bf16[768,2048]{1,0:T(8,128)(2,1)}, u32[]{:S(2)}) copy-start(bf16[768,2048]{1,0:T(8,128)(2,1)} %param.26) | copy-start | bytes 9437188
  6.5 69.6 %all-gather.5.cloned.1.call-start = ((), (), s32[]{:S(2)}) async-start(), calls=%async_computation.7 | async-start | bytes 1064960 | tf_op jit(solution)/shard_map/all_gather | solution.py:133
  8.2 147.3 %all-gather.3.cloned.1.call-start = ((), (), s32[]{:S(2)}) async-start(), calls=%async_computation.6 | async-start | bytes 8519680 | tf_op jit(solution)/shard_map/all_gather | solution.py:132
  10.3 21.1 %all-to-all-start = ((s32[64,256,1]{1,2,0:T(1,128)}), s32[64,256,1]{1,2,0:T(1,128)S(1)}, u32[]{:S(2)}, u32[]{:S(2)}) async-start(s32[64,256,1]{1,2,0:T(1,128)} %concatenate.12), calls=%async_computation | async-start | bytes 131072 | tf_op jit(solution)/shard_map/all_to_all | solution.py:18
  25.5 130.0 %copy-start.15 = (s32[256]{0:T(256)}, s32[256]{0:T(256)S(1)}, u32[]{:S(2)}) copy-start(s32[256]{0:T(256)S(1)} %fusion.49) | copy-start | bytes 3076
  31.4 124.1 %copy-start.12 = (s32[64,256,1]{1,2,0:T(1,128)}, s32[64,256,1]{1,2,0:T(1,128)S(1)}, u32[]{:S(2)}) copy-start(s32[64,256,1]{1,2,0:T(1,128)S(1)} %all-to-all-done) | copy-start | bytes 196612
  161.9 2.9 copy-start.11
  161.9 2.9 copy-start.10
  161.9 2.9 copy-start.13
  161.9 2.9 copy-start.14
  161.9 3.1 copy-start.4
  365.4 6.5 %copy-start.17 = (f32[2048]{0:T(1024)S(1)}, f32[2048]{0:T(1024)}, u32[]{:S(2)}) copy-start(f32[2048]{0:T(1024)} %param.27) | copy-start | bytes 24580
  367.1 4.8 copy-start.6
  371.2 1.7 copy-start.7
  371.2 1.7 copy-start.18
  517.4 7.2 %copy-start.20 = (bf16[1,2048,512]{2,1,0:T(8,128)(2,1)S(1)}, bf16[1,2048,512]{2,1,0:T(8,128)(2,1)}, u32[]{:S(2)}) copy-start(bf16[1,2048,512]{2,1,0:T(8,128)(2,1)} %param.32) | copy-start | bytes 6291460
  524.7 2.3 copy-start.21
  527.0 2.7 copy-start.22
  546.7 6.1 %copy-start.8 = (s32[128,2]{1,0:T(8,128)S(1)}, s32[128,2]{1,0:T(8,128)}, u32[]{:S(2)}) copy-start(s32[128,2]{1,0:T(8,128)} %get-tuple-element.385) | copy-start | bytes 3076
  546.8 6.2 %copy-start.19 = (f32[128,2]{0,1:T(2,128)S(1)}, f32[128,2]{0,1:T(2,128)}, u32[]{:S(2)}) copy-start(f32[128,2]{0,1:T(2,128)} %param.30) | copy-start | bytes 3076
  546.8 6.4 %copy-start.16 = (s32[256]{0:T(256)S(1)}, s32[256]{0:T(256)}, u32[]{:S(2)}) copy-start(s32[256]{0:T(256)} %copy-done.15) | copy-start | bytes 3076
  546.8 36.2 %all-to-all-start.5 = ((bf16[64,8,2048]{2,1,0:T(8,128)(2,1)}), bf16[64,8,2048]{2,1,0:T(8,128)(2,1)S(1)}, u32[]{:S(2)}, u32[]{:S(2)}) async-start(bf16[64,8,2048]{2,1,0:T(8,128)(2,1)} %copy.67), calls=%async_computation.5 | async-start | bytes 4194304 | tf_op jit(solution)/shard_map/all_to_all | solution.py:204
  585.3 9.3 %copy-start.1 = (bf16[768,2048]{1,0:T(8,128)(2,1)S(1)}, bf16[768,2048]{1,0:T(8,128)(2,1)}, u32[]{:S(2)}) copy-start(bf16[768,2048]{1,0:T(8,128)(2,1)} %param.26) | copy-start | bytes 9437188
  588.9 4.9 copy-start.3
  (34 other events, 20.8 us)
Sparse Core Ops, SparseCore 0:
  10.0 66.1 all-gather.4
  79.0 76.4 all-gather.2
